TPU v7x, 32 devices: a whole 2x2x4 slice. The times are simulated.
32 devices in a mesh: pp: 4 (over z), fs: 2 (over y), tp: 4 (over x, core).
Axes of the slice: x: 2, y: 2, z: 4, core: 2. Of those that a mesh axis runs over, the one named last changes fastest.
Arguments:
- tokens_in: bfloat16 [4, 8, 8, 2048], P('pp', ('fs', 'tp')), may hold values from -6 to 6
- weight_in: bfloat16 [4, 2048, 512], P('pp'), may hold values from -0.125 to 0.125
- conv_taps: float32 [4, 4, 512], P('pp'), may hold values from -3 to 3
- conv_bias: float32 [4, 512], P('pp'), may hold values from -2 to 2
- gate_rate: bfloat16 [4, 8, 64, 64], P('pp'), may hold values from -0.75 to 0.75
- bias_rate: float32 [4, 512], P('pp'), may hold values from -3 to 3
- gate_input: bfloat16 [4, 8, 64, 64], P('pp'), may hold values from -0.75 to 0.75
- bias_input: float32 [4, 512], P('pp'), may hold values from -3 to 3
- decay_param: float32 [4, 512], P('pp'), may hold values from 3.5 to 7.5
- weight_out: bfloat16 [4, 512, 2048], P('pp'), may hold values from -0.5 to 0.5
- norm_gain: float32 [4, 2048], P('pp'), may hold values from 0.1 to 1.9
- norm_shift: float32 [4, 2048], P('pp'), may hold values from -2 to 2
Outputs:
- tokens_out: bfloat16 [4, 8, 8, 2048], P('pp', ('fs', 'tp'))
All inputs are finite; a program needn't handle non-finite values.
Results may differ from a plain program's by a relative error of at most 0.022.
Values may be sent and summed in bfloat16 or wider, within the bound.
A program may use at most 128 MiB of HBM per device.

v0:
```python
import jax
import jax.numpy as jnp
from jax import lax
from jax.sharding import PartitionSpec as P

decay_scale = 8.0
norm_eps = 1e-05


def passed_along(x, axis, by):
    length = lax.axis_size(axis)
    pairs = [(i, i + by) for i in range(length) if 0 <= i + by < length]
    return lax.ppermute(x, axis, pairs)


def combine_steps(earlier, later):
    return (earlier[0] * later[0], later[0] * earlier[1] + later[1])


def recurrence(
    projected, conv_taps, conv_bias, gate_rate, bias_rate, gate_input, bias_input, decay_param
):
    seq_count, length, channels = projected.shape
    tap_count = conv_taps.shape[0]
    padded = jnp.pad(projected.astype(jnp.float32), ((0, 0), (tap_count - 1, 0), (0, 0)))
    convolved = conv_bias + padded[:, 0:length] * conv_taps[0]
    for tap_index in range(1, tap_count):
        convolved = convolved + padded[:, tap_index : tap_index + length] * conv_taps[tap_index]
    convolved = convolved.astype(jnp.bfloat16)
    blocks = gate_rate.shape[0]
    block_width = gate_rate.shape[1]
    grouped = convolved.reshape(seq_count, length, blocks, block_width)
    rate_pre = jnp.einsum("bsnc,ncd->bsnd", grouped, gate_rate, preferred_element_type=jnp.float32)
    input_pre = jnp.einsum(
        "bsnc,ncd->bsnd", grouped, gate_input, preferred_element_type=jnp.float32
    )
    rate_gate = jax.nn.sigmoid(rate_pre.reshape(seq_count, length, channels) + bias_rate)
    input_gate = jax.nn.sigmoid(input_pre.reshape(seq_count, length, channels) + bias_input)
    log_decay = -decay_scale * rate_gate * jax.nn.softplus(-decay_param)
    scale_in = jnp.sqrt(-jnp.expm1(2.0 * log_decay))
    driven = scale_in * input_gate * convolved.astype(jnp.float32)
    decay_now = jnp.exp(log_decay)
    unused, hidden = lax.associative_scan(combine_steps, (decay_now, driven), axis=1)
    return hidden.astype(jnp.bfloat16)


def shards(
    tokens_in,
    weight_in,
    conv_taps,
    conv_bias,
    gate_rate,
    bias_rate,
    gate_input,
    bias_input,
    decay_param,
    weight_out,
    norm_gain,
    norm_shift,
):
    section_count = lax.axis_size("pp")
    section_index = lax.axis_index("pp")
    micro_count = section_count // 2
    length = tokens_in.shape[2]
    model_width = tokens_in.shape[3]
    w_project = weight_in[0]
    w_back = weight_out[0]
    lru_width = w_project.shape[1]

    def section_apply(entry_rows, is_valid):
        pair_count = entry_rows.shape[0]
        flat_rows = entry_rows.reshape(pair_count * length, model_width)

        def run_section():
            projected = jnp.dot(flat_rows, w_project, preferred_element_type=jnp.float32).astype(
                jnp.bfloat16
            )
            mixed_out = recurrence(
                projected.reshape(pair_count, length, lru_width),
                conv_taps[0],
                conv_bias[0],
                gate_rate[0],
                bias_rate[0],
                gate_input[0],
                bias_input[0],
                decay_param[0],
            )
            summed = flat_rows.astype(jnp.float32) + jnp.dot(
                mixed_out.reshape(pair_count * length, lru_width),
                w_back,
                preferred_element_type=jnp.float32,
            )
            mean_value = jnp.mean(summed, axis=-1, keepdims=True)
            centered = summed - mean_value
            variance = jnp.mean(centered * centered, axis=-1, keepdims=True)
            normed = centered * lax.rsqrt(variance + norm_eps) * norm_gain[0] + norm_shift[0]
            return normed.astype(jnp.bfloat16).reshape(pair_count, length, model_width)

        return lax.cond(
            is_valid,
            run_section,
            lambda: jnp.zeros((pair_count, length, model_width), jnp.bfloat16),
        )

    def advance(step_index, moving, out_buffer, first_input):
        entry_rows = jnp.where(section_index == 0, first_input, moving)
        offset = step_index - section_index
        is_valid = (offset >= 0) & (offset < micro_count)
        result = section_apply(entry_rows, is_valid)
        moving_next = passed_along(result, "pp", 1)
        out_slot = jnp.clip(step_index - (section_count - 1), 0, micro_count - 1).astype(jnp.int32)
        do_write = (section_index == section_count - 1) & (step_index >= section_count - 1)
        current = lax.dynamic_index_in_dim(out_buffer, out_slot, 0, keepdims=False)
        out_buffer = lax.dynamic_update_index_in_dim(
            out_buffer, jnp.where(do_write, result, current), out_slot, 0
        )
        return (moving_next, out_buffer)

    blank_rows = jnp.zeros((2, length, model_width), jnp.bfloat16)
    out_buffer = jnp.zeros((micro_count, 2, length, model_width), jnp.bfloat16)
    everyone = lax.all_gather(tokens_in, "pp", axis=0, tiled=True)

    def feed_turn(step_index, state_pair):
        first_input = lax.dynamic_slice_in_dim(everyone, 2 * step_index, 2, 0).reshape(
            2, length, model_width
        )
        return advance(step_index, state_pair[0], state_pair[1], first_input)

    moving, out_buffer = lax.fori_loop(0, micro_count, feed_turn, (blank_rows, out_buffer))

    def drain_turn(step_index, state_pair):
        return advance(step_index, state_pair[0], state_pair[1], state_pair[0])

    moving, out_buffer = lax.fori_loop(
        micro_count, micro_count + section_count - 1, drain_turn, (moving, out_buffer)
    )
    by_slot = out_buffer.reshape(section_count, length, model_width)
    arrived = lax.all_to_all(by_slot, "pp", split_axis=0, concat_axis=0, tiled=True)
    own_entry = arrived[section_count - 1 : section_count]
    return own_entry.reshape(1, 1, length, model_width)


def solution(mesh):
    placed = (
        P("pp", ("fs", "tp"), None, None),
        P("pp", None, None),
        P("pp", None, None),
        P("pp", None),
        P("pp", None, None, None),
        P("pp", None),
        P("pp", None, None, None),
        P("pp", None),
        P("pp", None),
        P("pp", None, None),
        P("pp", None),
        P("pp", None),
    )
    return jax.shard_map(
        shards,
        mesh=mesh,
        in_specs=placed,
        out_specs=P("pp", ("fs", "tp"), None, None),
        check_vma=False,
    )
```

profile of v0, /device:TPU:0, one launch (start us, length us, event | category | flops | bytes accessed | tf_op | source)
XLA Modules:
  0.0 77.0 jit_solution(6540700133012021219)
XLA Ops:
  0.0 15.3 %all_gather.3 = bf16[4,1,8,2048]{3,2,1,0:T(8,128)(2,1)S(1)} all-gather(bf16[1,1,8,2048]{3,2,1,0:T(8,128)(2,1)} %param.20), channel_id=1, replica_groups=mesh['pp'=4,'fs'=2,'tp'=4] {'pp'}, dimensions={0}, use_global_device_ids=true | all-gather | bytes 163840 | tf_op jit(solution)/shard_map/all_gather | solution.py:121
  15.3 18.3 %while.36 = (s32[]{:T(128)}, bf16[2,8,2048]{2,1,0:T(8,128)(2,1)S(1)}, bf16[2,2,8,2048]{3,2,1,0:T(8,128)(2,1)S(1)}, s32[]{:T(128)}, pred[]{:T(512)}, /*index=5*/b...) while((s32[]{:T(128)}, ...), condition=%wide.region_5.6_spmd, body=%wide.region_0.5_spmd.sunk | while | flops 70007832 | bytes 16215412 | solution.py:129
  15.3 4.5 %conditional.4 = (bf16[2,8,2048]{2,1,0:T(8,128)(2,1)S(1)}) conditional(s32[]{:T(128)} %convert_element_type.130, () %tuple.117, (pred[]{:T(512)}, s32[]{:T(128)}, bf16[4,1,8,2048]{3,2,0,1:T(8,128)(2,1)S(1)}, bf16[2,8,2048]{2,1,0:T(8,128)(2,1)S(1)}, f32[1,512]{1,0:T(1,128)}, /*index=5*/bf16[2048,512]{1,0:T(8,128)(2,1)}, f32[1,4,512]{2,1,0:T(4,128)}, ...), branch_computations={%region_1.1_spmd, %region_2.4_spmd} | conditional | flops 69975056 | bytes 15625128 | solution.py:99
  15.4 0.0 copy-start.8
  15.4 0.0 copy-start.6
  15.4 0.0 copy-start.2
  15.4 0.0 copy-start.4
  15.4 0.0 copy-start.17
  15.4 0.0 copy-start.13
  15.4 0.0 copy-start.15
  15.5 0.0 copy-start
  15.5 2.1 %fusion.1 = f32[2,8,512]{2,1,0:T(8,128)S(1)} fusion(bf16[2048,512]{1,0:T(8,128)(2,1)} %get-tuple-element.995, bf16[2,8,2048]{2,1,0:T(8,128)(2,1)S(1)} %get-tuple-element.993, bf16[4,1,8,2048]{3,2,0,1:T(8,128)(2,1)S(1)} %get-tuple-element.991, s32[]{:T(128)S(6)} %select_n.106, pred[]{:T(512)} %get-tuple-element.990), kind=kOutput, calls=%fused_computation.5 | convolution fusion | flops 33603584 | bytes 2260997 | tf_op jit(solution)/shard_map/while/body/eval_jaxpr/cond/branch_1_fun/dot_general | solution.py:75
  17.7 0.1 reshape.150
  17.8 0.1 convolution_bitcast_fusion.1
  17.9 0.0 copy-start.9
  18.0 0.1 reshape.151
  18.0 0.1 convolution_bitcast_fusion
  18.2 0.1 reshape.152
  18.3 0.1 fusion.23
  19.0 0.5 fusion.52
  19.5 0.2 multiply_reduce_fusion
  19.7 0.1 fusion.4
  19.8 1.3 %collective-permute-start = (bf16[2,8,2048]{2,1,0:T(8,128)(2,1)S(1)}, bf16[2,8,2048]{2,1,0:T(8,128)(2,1)S(1)}, u32[]{:S(2)}, u32[]{:S(2)}) collective-permute-start(bf16[2,8,2048]{2,1,0:T(8,128)(2,1)S(1)} %get-tuple-element.1515), channel_id=1, source_target_pairs={{0,8},{8,16},{16,24},{1,9},{9,17},{17,25},{2,10},{10,18},{18,26},{... | collective-permute-start | bytes 196616 | tf_op jit(solution)/shard_map/while/body/eval_jaxpr/ppermute | solution.py:13
  21.2 1.8 %collective-permute-done = bf16[2,8,2048]{2,1,0:T(8,128)(2,1)S(1)} collective-permute-done((bf16[2,8,2048]{2,1,0:T(8,128)(2,1)S(1)}, bf16[2,8,2048]{2,1,0:T(8,128)(2,1)S(1)}, u32[]{:S(2)}, u32[]{:S(2)}) %collective-permute-start) | collective-permute-done | bytes 65568 | tf_op jit(solution)/shard_map/while/body/eval_jaxpr/ppermute | solution.py:13
  23.0 4.4 %conditional.4 = (bf16[2,8,2048]{2,1,0:T(8,128)(2,1)S(1)}) conditional(s32[]{:T(128)} %convert_element_type.130, () %tuple.117, (pred[]{:T(512)}, s32[]{:T(128)}, bf16[4,1,8,2048]{3,2,0,1:T(8,128)(2,1)S(1)}, bf16[2,8,2048]{2,1,0:T(8,128)(2,1)S(1)}, f32[1,512]{1,0:T(1,128)}, /*index=5*/bf16[2048,512]{1,0:T(8,128)(2,1)}, f32[1,4,512]{2,1,0:T(4,128)}, ...), branch_computations={%region_1.1_spmd, %region_2.4_spmd} | conditional | flops 69975056 | bytes 15625128 | solution.py:99
  23.0 0.0 copy-start.15
  23.1 0.0 copy-start
  23.1 2.1 %fusion.1 = f32[2,8,512]{2,1,0:T(8,128)S(1)} fusion(bf16[2048,512]{1,0:T(8,128)(2,1)} %get-tuple-element.995, bf16[2,8,2048]{2,1,0:T(8,128)(2,1)S(1)} %get-tuple-element.993, bf16[4,1,8,2048]{3,2,0,1:T(8,128)(2,1)S(1)} %get-tuple-element.991, s32[]{:T(128)S(6)} %select_n.106, pred[]{:T(512)} %get-tuple-element.990), kind=kOutput, calls=%fused_computation.5 | convolution fusion | flops 33603584 | bytes 2260997 | tf_op jit(solution)/shard_map/while/body/eval_jaxpr/cond/branch_1_fun/dot_general | solution.py:75
  25.3 0.1 reshape.150
  25.4 0.1 convolution_bitcast_fusion.1
  25.6 0.1 reshape.151
  25.7 0.1 convolution_bitcast_fusion
  25.8 0.1 reshape.152
  26.0 0.1 fusion.23
  26.6 0.5 fusion.52
  27.1 0.2 multiply_reduce_fusion
  27.3 0.1 fusion.4
  27.4 4.3 %collective-permute-start = (bf16[2,8,2048]{2,1,0:T(8,128)(2,1)S(1)}, bf16[2,8,2048]{2,1,0:T(8,128)(2,1)S(1)}, u32[]{:S(2)}, u32[]{:S(2)}) collective-permute-start(bf16[2,8,2048]{2,1,0:T(8,128)(2,1)S(1)} %get-tuple-element.1515), channel_id=1, source_target_pairs={{0,8},{8,16},{16,24},{1,9},{9,17},{17,25},{2,10},{10,18},{18,26},{... | collective-permute-start | bytes 196616 | tf_op jit(solution)/shard_map/while/body/eval_jaxpr/ppermute | solution.py:13
  31.8 1.8 %collective-permute-done = bf16[2,8,2048]{2,1,0:T(8,128)(2,1)S(1)} collective-permute-done((bf16[2,8,2048]{2,1,0:T(8,128)(2,1)S(1)}, bf16[2,8,2048]{2,1,0:T(8,128)(2,1)S(1)}, u32[]{:S(2)}, u32[]{:S(2)}) %collective-permute-start) | collective-permute-done | bytes 65568 | tf_op jit(solution)/shard_map/while/body/eval_jaxpr/ppermute | solution.py:13
  33.6 26.6 %while.37 = (s32[]{:T(128)}, bf16[2,8,2048]{2,1,0:T(8,128)(2,1)S(1)}, bf16[2,2,8,2048]{3,2,1,0:T(8,128)(2,1)S(1)}, s32[]{:T(128)}, f32[1,512]{1,0:T(1,128)}, /*i...) while((s32[]{:T(128)}, ...), condition=%wide.region_11.12_spmd, body=%wide.region_6.11_spmd.sunk | while | flops 69942296 | bytes 16051460 | solution.py:134
  33.6 9.5 %collective-permute-start.1 = (bf16[2,8,2048]{2,1,0:T(8,128)(2,1)S(1)}, bf16[2,8,2048]{2,1,0:T(8,128)(2,1)S(1)}, u32[]{:S(2)}, u32[]{:S(2)}) collective-permute-start(bf16[2,8,2048]{2,1,0:T(8,128)(2,1)S(1)} %get-tuple-element.1516), channel_id=1, source_target_pairs={{0,8},{8,16},{16,24},{1,9},{9,17},{17,25},{2,10},{10,18},{18,26},{... | collective-permute-start | bytes 196616 | tf_op jit(solution)/shard_map/while/body/eval_jaxpr/ppermute | solution.py:13
  43.2 1.9 %collective-permute-done.1 = bf16[2,8,2048]{2,1,0:T(8,128)(2,1)S(1)} collective-permute-done((bf16[2,8,2048]{2,1,0:T(8,128)(2,1)S(1)}, bf16[2,8,2048]{2,1,0:T(8,128)(2,1)S(1)}, u32[]{:S(2)}, u32[]{:S(2)}) %collective-permute-start.1) | collective-permute-done | bytes 65568 | tf_op jit(solution)/shard_map/while/body/eval_jaxpr/ppermute | solution.py:13
  45.1 4.4 %collective-permute-start.1 = (bf16[2,8,2048]{2,1,0:T(8,128)(2,1)S(1)}, bf16[2,8,2048]{2,1,0:T(8,128)(2,1)S(1)}, u32[]{:S(2)}, u32[]{:S(2)}) collective-permute-start(bf16[2,8,2048]{2,1,0:T(8,128)(2,1)S(1)} %get-tuple-element.1516), channel_id=1, source_target_pairs={{0,8},{8,16},{16,24},{1,9},{9,17},{17,25},{2,10},{10,18},{18,26},{... | collective-permute-start | bytes 196616 | tf_op jit(solution)/shard_map/while/body/eval_jaxpr/ppermute | solution.py:13
  49.6 1.8 %collective-permute-done.1 = bf16[2,8,2048]{2,1,0:T(8,128)(2,1)S(1)} collective-permute-done((bf16[2,8,2048]{2,1,0:T(8,128)(2,1)S(1)}, bf16[2,8,2048]{2,1,0:T(8,128)(2,1)S(1)}, u32[]{:S(2)}, u32[]{:S(2)}) %collective-permute-start.1) | collective-permute-done | bytes 65568 | tf_op jit(solution)/shard_map/while/body/eval_jaxpr/ppermute | solution.py:13
  51.4 6.9 %collective-permute-start.1 = (bf16[2,8,2048]{2,1,0:T(8,128)(2,1)S(1)}, bf16[2,8,2048]{2,1,0:T(8,128)(2,1)S(1)}, u32[]{:S(2)}, u32[]{:S(2)}) collective-permute-start(bf16[2,8,2048]{2,1,0:T(8,128)(2,1)S(1)} %get-tuple-element.1516), channel_id=1, source_target_pairs={{0,8},{8,16},{16,24},{1,9},{9,17},{17,25},{2,10},{10,18},{18,26},{... | collective-permute-start | bytes 196616 | tf_op jit(solution)/shard_map/while/body/eval_jaxpr/ppermute | solution.py:13
  58.4 1.8 %collective-permute-done.1 = bf16[2,8,2048]{2,1,0:T(8,128)(2,1)S(1)} collective-permute-done((bf16[2,8,2048]{2,1,0:T(8,128)(2,1)S(1)}, bf16[2,8,2048]{2,1,0:T(8,128)(2,1)S(1)}, u32[]{:S(2)}, u32[]{:S(2)}) %collective-permute-start.1) | collective-permute-done | bytes 65568 | tf_op jit(solution)/shard_map/while/body/eval_jaxpr/ppermute | solution.py:13
  60.2 16.2 %all_to_all.5 = bf16[4,8,2048]{2,1,0:T(8,128)(2,1)S(1)} all-to-all(bf16[4,8,2048]{2,1,0:T(8,128)(2,1)S(1)} %bitcast.143), channel_id=1, replica_groups=mesh['pp'=4,'fs'=2,'tp'=4] {'pp'}, dimensions={0} | all-to-all | bytes 262144 | tf_op jit(solution)/shard_map/all_to_all | solution.py:138
  76.3 0.6 slice_bitcast_fusion
  (111 shorter events, 1.5 us)
Async XLA Ops:
  15.4 2.2 %copy-start.8 = (f32[1,4,512]{2,1,0:T(4,128)S(1)}, f32[1,4,512]{2,1,0:T(4,128)}, u32[]{:S(2)}) copy-start(f32[1,4,512]{2,1,0:T(4,128)} %get-tuple-element.996) | copy-start | bytes 24580 | tf_op jit(solution)/shard_map/while/body/eval_jaxpr/cond
  15.4 2.2 %copy-start.6 = (f32[1,512]{1,0:T(1,128)S(1)}, f32[1,512]{1,0:T(1,128)}, u32[]{:S(2)}) copy-start(f32[1,512]{1,0:T(1,128)} %get-tuple-element.994) | copy-start | bytes 6148 | tf_op jit(solution)/shard_map/while/body/eval_jaxpr/cond
  15.4 2.4 %copy-start.2 = (bf16[1,8,64,64]{3,2,1,0:T(8,128)(2,1)S(1)}, bf16[1,8,64,64]{3,2,1,0:T(8,128)(2,1)}, u32[]{:S(2)}) copy-start(bf16[1,8,64,64]{3,2,1,0:T(8,128)(2,1)} %get-tuple-element.997) | copy-start | bytes 196612 | tf_op jit(solution)/shard_map/while/body/eval_jaxpr/cond
  15.4 2.6 %copy-start.4 = (bf16[1,8,64,64]{3,2,1,0:T(8,128)(2,1)S(1)}, bf16[1,8,64,64]{3,2,1,0:T(8,128)(2,1)}, u32[]{:S(2)}) copy-start(bf16[1,8,64,64]{3,2,1,0:T(8,128)(2,1)} %get-tuple-element.1000) | copy-start | bytes 196612 | tf_op jit(solution)/shard_map/while/body/eval_jaxpr/cond
  15.4 2.9 %copy-start.17 = (f32[1,512]{1,0:T(1,128)S(1)}, f32[1,512]{1,0:T(1,128)}, u32[]{:S(2)}) copy-start(f32[1,512]{1,0:T(1,128)} %get-tuple-element.999) | copy-start | bytes 6148 | tf_op jit(solution)/shard_map/while/body/eval_jaxpr/cond
  15.4 2.9 %copy-start.13 = (f32[1,512]{1,0:T(1,128)S(1)}, f32[1,512]{1,0:T(1,128)}, u32[]{:S(2)}) copy-start(f32[1,512]{1,0:T(1,128)} %get-tuple-element.998) | copy-start | bytes 6148 | tf_op jit(solution)/shard_map/while/body/eval_jaxpr/cond
  15.4 2.9 %copy-start.15 = (f32[1,512]{1,0:T(1,128)S(1)}, f32[1,512]{1,0:T(1,128)}, u32[]{:S(2)}) copy-start(f32[1,512]{1,0:T(1,128)} %get-tuple-element.1001) | copy-start | bytes 6148 | tf_op jit(solution)/shard_map/while/body/eval_jaxpr/cond
  15.5 3.5 %copy-start = (bf16[512,2048]{1,0:T(8,128)(2,1)S(1)}, bf16[512,2048]{1,0:T(8,128)(2,1)}, u32[]{:S(2)}) copy-start(bf16[512,2048]{1,0:T(8,128)(2,1)} %get-tuple-element.1002) | copy-start | bytes 6291460 | tf_op jit(solution)/shard_map/while/body/eval_jaxpr/cond
  17.9 1.8 %copy-start.9 = (f32[1,2048]{1,0:T(1,128)S(1)}, f32[1,2048]{1,0:T(1,128)}, u32[]{:S(2)}) copy-start(f32[1,2048]{1,0:T(1,128)} %get-tuple-element.1003) | copy-start | bytes 24580 | tf_op jit(solution)/shard_map/while/body/eval_jaxpr/cond
  17.9 1.8 %copy-start.11 = (f32[1,2048]{1,0:T(1,128)S(1)}, f32[1,2048]{1,0:T(1,128)}, u32[]{:S(2)}) copy-start(f32[1,2048]{1,0:T(1,128)} %get-tuple-element.1004) | copy-start | bytes 24580 | tf_op jit(solution)/shard_map/while/body/eval_jaxpr/cond
  19.8 3.2 %collective-permute-start = (bf16[2,8,2048]{2,1,0:T(8,128)(2,1)S(1)}, bf16[2,8,2048]{2,1,0:T(8,128)(2,1)S(1)}, u32[]{:S(2)}, u32[]{:S(2)}) collective-permute-start(bf16[2,8,2048]{2,1,0:T(8,128)(2,1)S(1)} %get-tuple-element.1515), channel_id=1, source_target_pairs={{0,8},{8,16},{16,24},{1,9},{9,17},{17,25},{2,10},{10,18},{18,26},{... | collective-permute-start | bytes 196616 | tf_op jit(solution)/shard_map/while/body/eval_jaxpr/ppermute | solution.py:13
  23.0 2.2 %copy-start.8 = (f32[1,4,512]{2,1,0:T(4,128)S(1)}, f32[1,4,512]{2,1,0:T(4,128)}, u32[]{:S(2)}) copy-start(f32[1,4,512]{2,1,0:T(4,128)} %get-tuple-element.996) | copy-start | bytes 24580 | tf_op jit(solution)/shard_map/while/body/eval_jaxpr/cond
  23.0 2.2 %copy-start.6 = (f32[1,512]{1,0:T(1,128)S(1)}, f32[1,512]{1,0:T(1,128)}, u32[]{:S(2)}) copy-start(f32[1,512]{1,0:T(1,128)} %get-tuple-element.994) | copy-start | bytes 6148 | tf_op jit(solution)/shard_map/while/body/eval_jaxpr/cond
  23.0 2.3 %copy-start.2 = (bf16[1,8,64,64]{3,2,1,0:T(8,128)(2,1)S(1)}, bf16[1,8,64,64]{3,2,1,0:T(8,128)(2,1)}, u32[]{:S(2)}) copy-start(bf16[1,8,64,64]{3,2,1,0:T(8,128)(2,1)} %get-tuple-element.997) | copy-start | bytes 196612 | tf_op jit(solution)/shard_map/while/body/eval_jaxpr/cond
  23.0 2.6 %copy-start.4 = (bf16[1,8,64,64]{3,2,1,0:T(8,128)(2,1)S(1)}, bf16[1,8,64,64]{3,2,1,0:T(8,128)(2,1)}, u32[]{:S(2)}) copy-start(bf16[1,8,64,64]{3,2,1,0:T(8,128)(2,1)} %get-tuple-element.1000) | copy-start | bytes 196612 | tf_op jit(solution)/shard_map/while/body/eval_jaxpr/cond
  23.0 2.9 %copy-start.17 = (f32[1,512]{1,0:T(1,128)S(1)}, f32[1,512]{1,0:T(1,128)}, u32[]{:S(2)}) copy-start(f32[1,512]{1,0:T(1,128)} %get-tuple-element.999) | copy-start | bytes 6148 | tf_op jit(solution)/shard_map/while/body/eval_jaxpr/cond
  23.0 2.9 %copy-start.13 = (f32[1,512]{1,0:T(1,128)S(1)}, f32[1,512]{1,0:T(1,128)}, u32[]{:S(2)}) copy-start(f32[1,512]{1,0:T(1,128)} %get-tuple-element.998) | copy-start | bytes 6148 | tf_op jit(solution)/shard_map/while/body/eval_jaxpr/cond
  23.0 2.9 %copy-start.15 = (f32[1,512]{1,0:T(1,128)S(1)}, f32[1,512]{1,0:T(1,128)}, u32[]{:S(2)}) copy-start(f32[1,512]{1,0:T(1,128)} %get-tuple-element.1001) | copy-start | bytes 6148 | tf_op jit(solution)/shard_map/while/body/eval_jaxpr/cond
  23.1 3.5 %copy-start = (bf16[512,2048]{1,0:T(8,128)(2,1)S(1)}, bf16[512,2048]{1,0:T(8,128)(2,1)}, u32[]{:S(2)}) copy-start(bf16[512,2048]{1,0:T(8,128)(2,1)} %get-tuple-element.1002) | copy-start | bytes 6291460 | tf_op jit(solution)/shard_map/while/body/eval_jaxpr/cond
  25.6 1.8 %copy-start.9 = (f32[1,2048]{1,0:T(1,128)S(1)}, f32[1,2048]{1,0:T(1,128)}, u32[]{:S(2)}) copy-start(f32[1,2048]{1,0:T(1,128)} %get-tuple-element.1003) | copy-start | bytes 24580 | tf_op jit(solution)/shard_map/while/body/eval_jaxpr/cond
  25.6 1.8 %copy-start.11 = (f32[1,2048]{1,0:T(1,128)S(1)}, f32[1,2048]{1,0:T(1,128)}, u32[]{:S(2)}) copy-start(f32[1,2048]{1,0:T(1,128)} %get-tuple-element.1004) | copy-start | bytes 24580 | tf_op jit(solution)/shard_map/while/body/eval_jaxpr/cond
  27.4 6.2 %collective-permute-start = (bf16[2,8,2048]{2,1,0:T(8,128)(2,1)S(1)}, bf16[2,8,2048]{2,1,0:T(8,128)(2,1)S(1)}, u32[]{:S(2)}, u32[]{:S(2)}) collective-permute-start(bf16[2,8,2048]{2,1,0:T(8,128)(2,1)S(1)} %get-tuple-element.1515), channel_id=1, source_target_pairs={{0,8},{8,16},{16,24},{1,9},{9,17},{17,25},{2,10},{10,18},{18,26},{... | collective-permute-start | bytes 196616 | tf_op jit(solution)/shard_map/while/body/eval_jaxpr/ppermute | solution.py:13
  33.6 11.5 %collective-permute-start.1 = (bf16[2,8,2048]{2,1,0:T(8,128)(2,1)S(1)}, bf16[2,8,2048]{2,1,0:T(8,128)(2,1)S(1)}, u32[]{:S(2)}, u32[]{:S(2)}) collective-permute-start(bf16[2,8,2048]{2,1,0:T(8,128)(2,1)S(1)} %get-tuple-element.1516), channel_id=1, source_target_pairs={{0,8},{8,16},{16,24},{1,9},{9,17},{17,25},{2,10},{10,18},{18,26},{... | collective-permute-start | bytes 196616 | tf_op jit(solution)/shard_map/while/body/eval_jaxpr/ppermute | solution.py:13
  45.1 6.3 %collective-permute-start.1 = (bf16[2,8,2048]{2,1,0:T(8,128)(2,1)S(1)}, bf16[2,8,2048]{2,1,0:T(8,128)(2,1)S(1)}, u32[]{:S(2)}, u32[]{:S(2)}) collective-permute-start(bf16[2,8,2048]{2,1,0:T(8,128)(2,1)S(1)} %get-tuple-element.1516), channel_id=1, source_target_pairs={{0,8},{8,16},{16,24},{1,9},{9,17},{17,25},{2,10},{10,18},{18,26},{... | collective-permute-start | bytes 196616 | tf_op jit(solution)/shard_map/while/body/eval_jaxpr/ppermute | solution.py:13
  51.4 8.8 %collective-permute-start.1 = (bf16[2,8,2048]{2,1,0:T(8,128)(2,1)S(1)}, bf16[2,8,2048]{2,1,0:T(8,128)(2,1)S(1)}, u32[]{:S(2)}, u32[]{:S(2)}) collective-permute-start(bf16[2,8,2048]{2,1,0:T(8,128)(2,1)S(1)} %get-tuple-element.1516), channel_id=1, source_target_pairs={{0,8},{8,16},{16,24},{1,9},{9,17},{17,25},{2,10},{10,18},{18,26},{... | collective-permute-start | bytes 196616 | tf_op jit(solution)/shard_map/while/body/eval_jaxpr/ppermute | solution.py:13
where the time goes:
time: 77.3 us; the launch traced here: 77 us
  blocking collectives  31.4 us (41%)
  starting transfers between devices  26.3 us (34%)
  waiting for transfers between devices  9.19 us (12%)
  matrix products  5.84 us (8%)
  local copies, waits for them, and re-layouts  2.18 us (3%)
  other arithmetic  1.21 us (2%)
    ppermute x5, starting transfers between devices, passed_along(): return lax.ppermute(x, axis, pairs)  26.3 us
    all_to_all x1, blocking collectives, shards(): lax.all_to_all(by_slot, 'pp', split_axis=0, concat_axis=0, tiled=True)  16.2 us
    all_gather x1, blocking collectives, shards(): everyone = lax.all_gather(tokens_in, 'pp', axis=0, tiled=True)  15.3 us
    ppermute x5, waiting for transfers between devices, passed_along(): return lax.ppermute(x, axis, pairs)  9.19 us
    dot_general x2, matrix products, run_section(): jnp.dot(flat_rows, w_project, preferred_element_type=jnp.float32)  4.25 us
  transfers between devices with their start and end apart: 5, of which 5 were waited for; matrix products, arithmetic and copies ran while one was open for 0% of the time, Pallas kernels for 0%

commit v1 on v0

v1 whole, which is shorter than its diff:
```python
import functools

import jax
import jax.numpy as jnp
from jax import lax
from jax.experimental import pallas as pl
from jax.experimental.pallas import tpu as pltpu
from jax.sharding import PartitionSpec as P

decay_scale = 8.0
norm_eps = 1e-05
mxu_width = 256
MESH = pl.DeviceIdType.MESH


def stack_kernel(
    sections,
    tokens_hbm,
    w_in_hbm,
    taps_hbm,
    cbias_hbm,
    grate_hbm,
    brate_hbm,
    ginput_hbm,
    binput_hbm,
    dparam_hbm,
    w_out_hbm,
    gain_hbm,
    shift_hbm,
    out_ref,
    w_in,
    w_out,
    taps,
    cbias,
    grate,
    brate,
    ginput,
    binput,
    dparam,
    gain,
    shift,
    rate_map,
    input_map,
    inbox,
    outbox,
    load_sem,
    entry_sem,
    send_sem,
    recv_sem,
    final_sem,
):
    section = lax.axis_index("pp")
    last = sections - 1
    length = inbox.shape[1]
    lru_width = w_in.shape[1]

    def other(offset):
        return lax.rem(section + offset, sections)

    barrier = pltpu.get_barrier_semaphore()
    for offset in range(1, sections):
        pl.semaphore_signal(
            barrier, inc=1, device_id={"pp": other(offset)}, device_id_type=MESH
        )

    def load(src, dst, index):
        return pltpu.make_async_copy(src, dst, load_sem.at[index])

    own = load(tokens_hbm.at[0, 0], inbox.at[0], 0)
    load_in = load(w_in_hbm.at[0], w_in, 1)
    load_out = load(w_out_hbm.at[0], w_out, 2)
    small = [
        load(grate_hbm.at[0], grate, 3),
        load(ginput_hbm.at[0], ginput, 4),
        load(taps_hbm.at[0], taps, 5),
        load(cbias_hbm, cbias, 6),
        load(brate_hbm, brate, 7),
        load(binput_hbm, binput, 8),
        load(dparam_hbm, dparam, 9),
        load(gain_hbm, gain, 10),
        load(shift_hbm, shift, 11),
    ]

    @pl.when(section == 0)
    def _():
        own.start()

    for copy in small:
        copy.start()
    load_in.start()
    load_out.start()

    for copy in small:
        copy.wait()
    blocks, block_width, _ = grate.shape
    group = max(1, min(blocks, mxu_width // block_width))
    wide = group * block_width
    rate_map[...] = jnp.zeros_like(rate_map)
    input_map[...] = jnp.zeros_like(input_map)
    for block in range(blocks):
        at = (block % group) * block_width
        rate_map[block // group, at : at + block_width, at : at + block_width] = grate[block]
        input_map[block // group, at : at + block_width, at : at + block_width] = ginput[block]
    minus_decay = -dparam[...]
    softplus = jnp.maximum(minus_decay, 0.0) + jnp.log1p(jnp.exp(-jnp.abs(minus_decay)))
    dparam[...] = -decay_scale * softplus

    entry = pltpu.make_async_remote_copy(
        src_ref=tokens_hbm.at[0, 0],
        dst_ref=inbox.at[section],
        send_sem=entry_sem,
        recv_sem=recv_sem.at[section],
        device_id={"pp": 0},
        device_id_type=MESH,
    )

    @pl.when(section > 0)
    def _():
        pl.semaphore_wait(barrier, sections - 1)
        entry.start()

    load_in.wait()
    load_out.wait()

    position = lax.broadcasted_iota(jnp.int32, (length, lru_width), 0)

    def delayed(x, by, fill):
        return jnp.where(position >= by, pltpu.roll(x, by, 0), fill)

    def onward(slot):
        return pltpu.make_async_remote_copy(
            src_ref=outbox.at[slot],
            dst_ref=inbox.at[slot],
            send_sem=send_sem.at[slot],
            recv_sem=recv_sem.at[slot],
            device_id={"pp": jnp.minimum(section + 1, last)},
            device_id_type=MESH,
        )

    def home(slot):
        return pltpu.make_async_remote_copy(
            src_ref=outbox.at[slot],
            dst_ref=out_ref.at[0, 0],
            send_sem=send_sem.at[slot],
            recv_sem=final_sem,
            device_id={"pp": slot},
            device_id_type=MESH,
        )

    def one_slot(slot, carry):
        from_here = (section == 0) & (slot == 0)

        @pl.when(from_here)
        def _():
            own.wait()

        @pl.when(jnp.logical_not(from_here))
        def _():
            onward(slot).wait_recv()

        stream = inbox[slot]
        projected = jnp.dot(stream, w_in[...], preferred_element_type=jnp.float32)
        projected = projected.astype(jnp.bfloat16).astype(jnp.float32)
        tap_count = taps.shape[0]
        convolved = cbias[...]
        for tap in range(tap_count):
            by = tap_count - 1 - tap
            shifted = delayed(projected, by, 0.0) if by else projected
            convolved = convolved + shifted * taps[tap : tap + 1]
        convolved = convolved.astype(jnp.bfloat16)

        def mapped(maps):
            return jnp.concatenate(
                [
                    jnp.dot(
                        convolved[:, i * wide : (i + 1) * wide],
                        maps[i],
                        preferred_element_type=jnp.float32,
                    )
                    for i in range(blocks // group)
                ],
                axis=1,
            )

        rate_gate = jax.nn.sigmoid(mapped(rate_map) + brate[...])
        input_gate = jax.nn.sigmoid(mapped(input_map) + binput[...])
        log_decay = rate_gate * dparam[...]
        decay = jnp.exp(log_decay)
        scale_in = jnp.sqrt(-jnp.tanh(log_decay) * (decay * decay + 1.0))
        hidden = scale_in * input_gate * convolved.astype(jnp.float32)
        by = 1
        while by < length:
            hidden = decay * delayed(hidden, by, 0.0) + hidden
            if 2 * by < length:
                decay = decay * delayed(decay, by, 1.0)
            by *= 2
        mixed = hidden.astype(jnp.bfloat16)
        summed = stream.astype(jnp.float32) + jnp.dot(
            mixed, w_out[...], preferred_element_type=jnp.float32
        )
        mean = jnp.mean(summed, axis=-1, keepdims=True)
        centered = summed - mean
        variance = jnp.mean(centered * centered, axis=-1, keepdims=True)
        normed = centered * lax.rsqrt(variance + norm_eps) * gain[...] + shift[...]
        result = normed.astype(jnp.bfloat16)
        outbox[slot] = result

        @pl.when(from_here)
        def _():
            pl.semaphore_wait(barrier, sections - 1)

        @pl.when(section < last)
        def _():
            onward(slot).start()

        @pl.when((section == last) & (slot < last))
        def _():
            home(slot).start()

        @pl.when((section == last) & (slot == last))
        def _():
            out_ref[0, 0] = outbox[slot]

        return carry

    lax.fori_loop(0, sections, one_slot, 0)

    @pl.when(section > 0)
    def _():
        entry.wait_send()

    @pl.when(section < last)
    def _():
        def sent(slot, carry):
            onward(slot).wait_send()
            return carry

        lax.fori_loop(0, sections, sent, 0)
        home(0).wait_recv()

    @pl.when(section == last)
    def _():
        def sent(slot, carry):
            home(slot).wait_send()
            return carry

        lax.fori_loop(0, last, sent, 0)


def shards(sections, tokens_in, *weights):
    _, _, length, width = tokens_in.shape
    lru_width = weights[0].shape[2]
    tap_count = weights[1].shape[1]
    _, blocks, block_width, _ = weights[3].shape
    group = max(1, min(blocks, mxu_width // block_width))
    wide = group * block_width
    vmem = pltpu.VMEM
    f32, bf16 = jnp.float32, jnp.bfloat16
    return pl.pallas_call(
        functools.partial(stack_kernel, sections),
        out_shape=jax.ShapeDtypeStruct(tokens_in.shape, tokens_in.dtype),
        in_specs=[pl.BlockSpec(memory_space=pl.ANY)] * (1 + len(weights)),
        out_specs=pl.BlockSpec(memory_space=pltpu.VMEM),
        scratch_shapes=[
            vmem((width, lru_width), bf16),
            vmem((lru_width, width), bf16),
            vmem((tap_count, lru_width), f32),
            vmem((1, lru_width), f32),
            vmem((blocks, block_width, block_width), bf16),
            vmem((1, lru_width), f32),
            vmem((blocks, block_width, block_width), bf16),
            vmem((1, lru_width), f32),
            vmem((1, lru_width), f32),
            vmem((1, width), f32),
            vmem((1, width), f32),
            vmem((blocks // group, wide, wide), bf16),
            vmem((blocks // group, wide, wide), bf16),
            vmem((sections, length, width), bf16),
            vmem((sections, length, width), bf16),
            pltpu.SemaphoreType.DMA((12,)),
            pltpu.SemaphoreType.DMA,
            pltpu.SemaphoreType.DMA((sections,)),
            pltpu.SemaphoreType.DMA((sections,)),
            pltpu.SemaphoreType.DMA,
        ],
        compiler_params=pltpu.CompilerParams(collective_id=0, has_side_effects=True),
        name="section_stack",
    )(tokens_in, *weights)


def solution(mesh):
    placed = (
        P("pp", ("fs", "tp"), None, None),
        P("pp", None, None),
        P("pp", None, None),
        P("pp", None),
        P("pp", None, None, None),
        P("pp", None),
        P("pp", None, None, None),
        P("pp", None),
        P("pp", None),
        P("pp", None, None),
        P("pp", None),
        P("pp", None),
    )
    return jax.shard_map(
        functools.partial(shards, mesh.shape["pp"]),
        mesh=mesh,
        in_specs=placed,
        out_specs=P("pp", ("fs", "tp"), None, None),
        check_vma=False,
    )
```

time: 77.3 us -> 25.6 us (0.33)
  the two profiles are of different devices: /device:TPU:0 before, /device:TPU:16 now
where the time goes in v1:
time: 25.6 us; the launch traced here: 25.4 us
  Pallas kernels  24.1 us (94%)
  local copies, waits for them, and re-layouts  1.38 us (5%)
    pallas_call x1, Pallas kernels, shards(): pl.pallas_call(functools.partial(stack_kernel, sections), out_shape=jax.S...  24.1 us
    unnamed x1, local copies, waits for them, and re-layouts  1.38 us

profile of v1, /device:TPU:16, one launch (start us, length us, event | category | flops | bytes accessed | tf_op | source)
XLA Modules:
  0.0 25.4 jit_solution(4191143309246173315)
XLA Ops:
  0.0 24.1 %section_stack.1 = bf16[1,1,8,2048]{3,2,1,0:T(8,128)(2,1)} custom-call(bf16[1,1,8,2048]{3,2,1,0:T(8,128)(2,1)} %tokens_hbm.1, bf16[1,2048,512]{2,1,0:T(8,128)(2,1)} %w_in_hbm.1, f32[1,4,512]{2,1,0:T(4,128)} %taps_hbm.1, f32[1,512]{1,0:T(1,128)} %cbias_hbm.1, bf16[1,8,64,64]{3,2,1,0:T(8,128)(2,1)} %grate_hbm.1, f32[1,512]{1,0:T(1,128)} %brate_hbm.1, ...), custom_call_target="tpu_custom_call" | custom-call | tf_op jit(solution)/shard_map/section_stack/pallas_call | solution.py:259
  24.1 1.4 %copy.14 = bf16[1,1,8,2048]{3,2,1,0:T(8,128)(2,1)} copy(bf16[1,1,8,2048]{3,2,1,0:T(8,128)(2,1)} %section_stack.1) | data formatting | bytes 65536

commit v2 on v1

v2 whole, which is shorter than its diff:
```python
import functools

import jax
import jax.numpy as jnp
from jax import lax
from jax.experimental import pallas as pl
from jax.experimental.pallas import tpu as pltpu
from jax.sharding import PartitionSpec as P

decay_scale = 8.0
norm_eps = 1e-05
mxu_width = 256
MESH = pl.DeviceIdType.MESH


def stack_kernel(
    sections,
    tokens_hbm,
    w_in_hbm,
    taps_hbm,
    cbias_hbm,
    grate_hbm,
    brate_hbm,
    ginput_hbm,
    binput_hbm,
    dparam_hbm,
    w_out_hbm,
    gain_hbm,
    shift_hbm,
    out_ref,
    w_in,
    w_out,
    taps,
    cbias,
    grate,
    brate,
    ginput,
    binput,
    dparam,
    gain,
    shift,
    rate_map,
    input_map,
    mine,
    inbox,
    outbox,
    load_sem,
    entry_sem,
    send_sem,
    recv_sem,
    final_sem,
):
    section = lax.axis_index("pp")
    column = lax.axis_index("tp")
    last = sections - 1
    pair, length = inbox.shape[1:3]
    lru_width = w_in.shape[1]
    core = lax.rem(column, pair)
    lead = pair - 1
    leads = core == lead
    first_stop = leads & (section == 0)
    last_stop = leads & (section == last)

    def at(stop, core_index):
        return {"pp": stop, "tp": column - core + core_index}

    barrier = pltpu.get_barrier_semaphore()

    def tell(stop, core_index):
        pl.semaphore_signal(
            barrier, inc=1, device_id=at(stop, core_index), device_id_type=MESH
        )

    @pl.when(first_stop)
    def _():
        for core_index in range(pair):
            for stop in range(sections):
                if (stop, core_index) != (0, lead):
                    tell(stop, core_index)

    @pl.when(jnp.logical_not(first_stop | last_stop))
    def _():
        tell(last, lead)

    @pl.when(leads & (section > 0))
    def _():
        @pl.when(section - 1 < last)
        def _():
            tell(section - 1, lead)

    heard = jnp.where(
        last_stop, sections * pair - 1, jnp.where(leads & (section > 0), 2, 1)
    ).astype(jnp.int32)

    def load(src, dst, index):
        return pltpu.make_async_copy(src, dst, load_sem.at[index])

    own = load(tokens_hbm.at[0, 0], mine, 0)
    load_in = load(w_in_hbm.at[0], w_in, 1)
    load_out = load(w_out_hbm.at[0], w_out, 2)
    small = [
        load(grate_hbm.at[0], grate, 3),
        load(ginput_hbm.at[0], ginput, 4),
        load(taps_hbm.at[0], taps, 5),
        load(cbias_hbm, cbias, 6),
        load(brate_hbm, brate, 7),
        load(binput_hbm, binput, 8),
        load(dparam_hbm, dparam, 9),
        load(gain_hbm, gain, 10),
        load(shift_hbm, shift, 11),
    ]
    own.start()

    @pl.when(leads)
    def _():
        for copy in small:
            copy.start()
        load_in.start()
        load_out.start()

    own.wait()
    entry = pltpu.make_async_remote_copy(
        src_ref=mine,
        dst_ref=inbox.at[section, core],
        send_sem=entry_sem,
        recv_sem=recv_sem.at[section, core],
        device_id=at(0, lead),
        device_id_type=MESH,
    )

    @pl.when(jnp.logical_not(first_stop))
    def _():
        pl.semaphore_wait(barrier, heard)
        entry.start()

    def entered(slot, core_index):
        return pltpu.make_async_remote_copy(
            src_ref=mine,
            dst_ref=inbox.at[slot, core_index],
            send_sem=entry_sem,
            recv_sem=recv_sem.at[slot, core_index],
            device_id=at(0, lead),
            device_id_type=MESH,
        )

    def onward(slot):
        return pltpu.make_async_remote_copy(
            src_ref=outbox.at[slot],
            dst_ref=inbox.at[slot],
            send_sem=send_sem.at[slot, 0],
            recv_sem=recv_sem.at[slot, 0],
            device_id=at(jnp.minimum(section + 1, last), lead),
            device_id_type=MESH,
        )

    def home(slot, core_index):
        return pltpu.make_async_remote_copy(
            src_ref=outbox.at[slot, core_index],
            dst_ref=out_ref.at[0, 0],
            send_sem=send_sem.at[slot, core_index],
            recv_sem=final_sem,
            device_id=at(slot, core_index),
            device_id_type=MESH,
        )

    def run_section():
        blocks, block_width, _ = grate.shape
        group = max(1, min(blocks, mxu_width // block_width))
        wide = group * block_width
        rate_map[...] = jnp.zeros_like(rate_map)
        input_map[...] = jnp.zeros_like(input_map)
        for copy in small:
            copy.wait()
        for block in range(blocks):
            to = (block % group) * block_width
            rate_map[block // group, to : to + block_width, to : to + block_width] = grate[block]
            input_map[block // group, to : to + block_width, to : to + block_width] = ginput[block]
        minus_decay = -dparam[...]
        softplus = jnp.maximum(minus_decay, 0.0) + jnp.log1p(jnp.exp(-jnp.abs(minus_decay)))
        dparam[...] = -decay_scale * softplus
        load_in.wait()
        load_out.wait()

        @pl.when(section == 0)
        def _():
            inbox[0, lead] = mine[...]

        position = lax.broadcasted_iota(jnp.int32, (pair, length, lru_width), 1)

        def delayed(x, by, fill):
            return jnp.where(position >= by, pltpu.roll(x, by, 1), fill)

        def one_slot(slot, carry):
            @pl.when(section == 0)
            def _():
                for core_index in range(pair):
                    if core_index == lead:
                        @pl.when(slot > 0)
                        def _():
                            entered(slot, core_index).wait_recv()
                    else:
                        entered(slot, core_index).wait_recv()

            @pl.when(section > 0)
            def _():
                onward(slot).wait_recv()

            rows = pair * length
            stream = inbox[slot].astype(jnp.float32).reshape(rows, -1)
            projected = jnp.dot(
                stream.astype(jnp.bfloat16), w_in[...], preferred_element_type=jnp.float32
            )
            projected = projected.astype(jnp.bfloat16).astype(jnp.float32)
            projected = projected.reshape(pair, length, lru_width)
            tap_count = taps.shape[0]
            convolved = cbias[...][None]
            for tap in range(tap_count):
                by = tap_count - 1 - tap
                shifted = delayed(projected, by, 0.0) if by else projected
                convolved = convolved + shifted * taps[tap : tap + 1][None]
            convolved = convolved.reshape(rows, lru_width).astype(jnp.bfloat16)

            def mapped(maps):
                return jnp.concatenate(
                    [
                        jnp.dot(
                            convolved[:, i * wide : (i + 1) * wide],
                            maps[i],
                            preferred_element_type=jnp.float32,
                        )
                        for i in range(blocks // group)
                    ],
                    axis=1,
                )

            rate_gate = jax.nn.sigmoid(mapped(rate_map) + brate[...])
            input_gate = jax.nn.sigmoid(mapped(input_map) + binput[...])
            log_decay = rate_gate * dparam[...]
            decay = jnp.exp(log_decay)
            scale_in = jnp.sqrt(-jnp.tanh(log_decay) * (decay * decay + 1.0))
            hidden = scale_in * input_gate * convolved.astype(jnp.float32)
            hidden = hidden.reshape(pair, length, lru_width)
            decay = decay.reshape(pair, length, lru_width)
            by = 1
            while by < length:
                hidden = decay * delayed(hidden, by, 0.0) + hidden
                if 2 * by < length:
                    decay = decay * delayed(decay, by, 1.0)
                by *= 2
            mixed = hidden.reshape(rows, lru_width).astype(jnp.bfloat16)
            summed = stream + jnp.dot(mixed, w_out[...], preferred_element_type=jnp.float32)
            mean = jnp.mean(summed, axis=-1, keepdims=True)
            centered = summed - mean
            variance = jnp.mean(centered * centered, axis=-1, keepdims=True)
            normed = centered * lax.rsqrt(variance + norm_eps) * gain[...] + shift[...]
            outbox[slot] = normed.reshape(pair, length, -1).astype(jnp.bfloat16)

            @pl.when((section == 0) & (slot == 0))
            def _():
                pl.semaphore_wait(barrier, heard)

            @pl.when(section < last)
            def _():
                onward(slot).start()

            @pl.when(section == last)
            def _():
                for core_index in range(pair):
                    if core_index == lead:
                        @pl.when(slot < last)
                        def _():
                            home(slot, core_index).start()

                        @pl.when(slot == last)
                        def _():
                            out_ref[0, 0] = outbox[slot, core_index]
                    else:
                        home(slot, core_index).start()

            return carry

        lax.fori_loop(0, sections, one_slot, 0)

        @pl.when(section < last)
        def _():
            def sent(slot, carry):
                onward(slot).wait_send()
                return carry

            lax.fori_loop(0, sections, sent, 0)

        @pl.when(section == last)
        def _():
            def sent(slot, carry):
                for core_index in range(pair):
                    if core_index == lead:
                        @pl.when(slot < last)
                        def _():
                            home(slot, core_index).wait_send()
                    else:
                        home(slot, core_index).wait_send()
                return carry

            lax.fori_loop(0, sections, sent, 0)

    pl.when(leads)(run_section)

    @pl.when(jnp.logical_not(first_stop))
    def _():
        entry.wait_send()

    @pl.when(jnp.logical_not(last_stop))
    def _():
        home(0, 0).wait_recv()


def shards(sections, pair, tokens_in, *weights):
    _, _, length, width = tokens_in.shape
    lru_width = weights[0].shape[2]
    tap_count = weights[1].shape[1]
    _, blocks, block_width, _ = weights[3].shape
    group = max(1, min(blocks, mxu_width // block_width))
    wide = group * block_width
    vmem = pltpu.VMEM
    f32, bf16 = jnp.float32, jnp.bfloat16
    return pl.pallas_call(
        functools.partial(stack_kernel, sections),
        out_shape=jax.ShapeDtypeStruct(tokens_in.shape, tokens_in.dtype),
        in_specs=[pl.BlockSpec(memory_space=pl.ANY)] * (1 + len(weights)),
        out_specs=pl.BlockSpec(memory_space=pltpu.VMEM),
        scratch_shapes=[
            vmem((width, lru_width), bf16),
            vmem((lru_width, width), bf16),
            vmem((tap_count, lru_width), f32),
            vmem((1, lru_width), f32),
            vmem((blocks, block_width, block_width), bf16),
            vmem((1, lru_width), f32),
            vmem((blocks, block_width, block_width), bf16),
            vmem((1, lru_width), f32),
            vmem((1, lru_width), f32),
            vmem((1, width), f32),
            vmem((1, width), f32),
            vmem((blocks // group, wide, wide), bf16),
            vmem((blocks // group, wide, wide), bf16),
            vmem((length, width), bf16),
            vmem((sections, pair, length, width), bf16),
            vmem((sections, pair, length, width), bf16),
            pltpu.SemaphoreType.DMA((12,)),
            pltpu.SemaphoreType.DMA,
            pltpu.SemaphoreType.DMA((sections, pair)),
            pltpu.SemaphoreType.DMA((sections, pair)),
            pltpu.SemaphoreType.DMA,
        ],
        compiler_params=pltpu.CompilerParams(collective_id=0, has_side_effects=True),
        name="section_stack",
    )(tokens_in, *weights)


def solution(mesh):
    placed = (
        P("pp", ("fs", "tp"), None, None),
        P("pp", None, None),
        P("pp", None, None),
        P("pp", None),
        P("pp", None, None, None),
        P("pp", None),
        P("pp", None, None, None),
        P("pp", None),
        P("pp", None),
        P("pp", None, None),
        P("pp", None),
        P("pp", None),
    )
    pair = 2 if mesh.shape["tp"] % 2 == 0 else 1
    return jax.shard_map(
        functools.partial(shards, mesh.shape["pp"], pair),
        mesh=mesh,
        in_specs=placed,
        out_specs=P("pp", ("fs", "tp"), None, None),
        check_vma=False,
    )
```

time: 25.6 us -> 21 us (0.82)
  the two profiles are of different devices: /device:TPU:16 before, /device:TPU:17 now
where the time goes in v2:
time: 21 us; the launch traced here: 20.8 us
  Pallas kernels  19.4 us (92%)
  local copies, waits for them, and re-layouts  1.38 us (7%)
    pallas_call x1, Pallas kernels, shards(): pl.pallas_call(functools.partial(stack_kernel, sections), out_shape=jax.S...  19.4 us
    unnamed x1, local copies, waits for them, and re-layouts  1.38 us

profile of v2, /device:TPU:17, one launch (start us, length us, event | category | flops | bytes accessed | tf_op | source)
XLA Modules:
  0.0 20.8 jit_solution(16946891814560603688)
XLA Ops:
  0.0 19.4 %section_stack.1 = bf16[1,1,8,2048]{3,2,1,0:T(8,128)(2,1)} custom-call(bf16[1,1,8,2048]{3,2,1,0:T(8,128)(2,1)} %tokens_hbm.1, bf16[1,2048,512]{2,1,0:T(8,128)(2,1)} %w_in_hbm.1, f32[1,4,512]{2,1,0:T(4,128)} %taps_hbm.1, f32[1,512]{1,0:T(1,128)} %cbias_hbm.1, bf16[1,8,64,64]{3,2,1,0:T(8,128)(2,1)} %grate_hbm.1, f32[1,512]{1,0:T(1,128)} %brate_hbm.1, ...), custom_call_target="tpu_custom_call" | custom-call | tf_op jit(solution)/shard_map/section_stack/pallas_call | solution.py:326
  19.4 1.4 %copy.14 = bf16[1,1,8,2048]{3,2,1,0:T(8,128)(2,1)} copy(bf16[1,1,8,2048]{3,2,1,0:T(8,128)(2,1)} %section_stack.1) | data formatting | bytes 65536

commit v3 on v2

--- a/solution.py
+++ b/solution.py
@@ -10,6 +10,7 @@
 decay_scale = 8.0
 norm_eps = 1e-05
 mxu_width = 256
+stream_parts = 4
 MESH = pl.DeviceIdType.MESH
 
 
@@ -48,13 +49,15 @@
     entry_sem,
     send_sem,
     recv_sem,
+    part_sem,
     final_sem,
 ):
     section = lax.axis_index("pp")
     column = lax.axis_index("tp")
     last = sections - 1
     pair, length = inbox.shape[1:3]
-    lru_width = w_in.shape[1]
+    width, lru_width = w_in.shape
+    parts = part_sem.shape[1]
     core = lax.rem(column, pair)
     lead = pair - 1
     leads = core == lead
@@ -143,12 +146,13 @@
             device_id_type=MESH,
         )
 
-    def onward(slot):
+    def onward(slot, part):
+        across = slice(part * width // parts, (part + 1) * width // parts)
         return pltpu.make_async_remote_copy(
-            src_ref=outbox.at[slot],
-            dst_ref=inbox.at[slot],
-            send_sem=send_sem.at[slot, 0],
-            recv_sem=recv_sem.at[slot, 0],
+            src_ref=outbox.at[slot, :, :, across],
+            dst_ref=inbox.at[slot, :, :, across],
+            send_sem=send_sem.at[slot, part],
+            recv_sem=part_sem.at[slot, part],
             device_id=at(jnp.minimum(section + 1, last), lead),
             device_id_type=MESH,
         )
@@ -201,15 +205,23 @@
                     else:
                         entered(slot, core_index).wait_recv()
 
-            @pl.when(section > 0)
-            def _():
-                onward(slot).wait_recv()
-
             rows = pair * length
-            stream = inbox[slot].astype(jnp.float32).reshape(rows, -1)
-            projected = jnp.dot(
-                stream.astype(jnp.bfloat16), w_in[...], preferred_element_type=jnp.float32
-            )
+            projected = jnp.zeros((rows, lru_width), jnp.float32)
+            streams = []
+            for part in range(parts):
+                @pl.when(section > 0)
+                def _():
+                    onward(slot, part).wait_recv()
+
+                across = slice(part * width // parts, (part + 1) * width // parts)
+                piece = inbox[slot, :, :, across].astype(jnp.float32).reshape(rows, -1)
+                streams.append(piece)
+                projected = projected + jnp.dot(
+                    piece.astype(jnp.bfloat16),
+                    w_in[across, :],
+                    preferred_element_type=jnp.float32,
+                )
+            stream = jnp.concatenate(streams, axis=1)
             projected = projected.astype(jnp.bfloat16).astype(jnp.float32)
             projected = projected.reshape(pair, length, lru_width)
             tap_count = taps.shape[0]
@@ -249,10 +261,11 @@
                 by *= 2
             mixed = hidden.reshape(rows, lru_width).astype(jnp.bfloat16)
             summed = stream + jnp.dot(mixed, w_out[...], preferred_element_type=jnp.float32)
-            mean = jnp.mean(summed, axis=-1, keepdims=True)
-            centered = summed - mean
-            variance = jnp.mean(centered * centered, axis=-1, keepdims=True)
-            normed = centered * lax.rsqrt(variance + norm_eps) * gain[...] + shift[...]
+            away = summed - jnp.mean(stream, axis=-1, keepdims=True)
+            offset = jnp.mean(away, axis=-1, keepdims=True)
+            square = jnp.mean(away * away, axis=-1, keepdims=True)
+            variance = jnp.maximum(square - offset * offset, 0.0)
+            normed = (away - offset) * lax.rsqrt(variance + norm_eps) * gain[...] + shift[...]
             outbox[slot] = normed.reshape(pair, length, -1).astype(jnp.bfloat16)
 
             @pl.when((section == 0) & (slot == 0))
@@ -261,7 +274,8 @@
 
             @pl.when(section < last)
             def _():
-                onward(slot).start()
+                for part in range(parts):
+                    onward(slot, part).start()
 
             @pl.when(section == last)
             def _():
@@ -284,7 +298,8 @@
         @pl.when(section < last)
         def _():
             def sent(slot, carry):
-                onward(slot).wait_send()
+                for part in range(parts):
+                    onward(slot, part).wait_send()
                 return carry
 
             lax.fori_loop(0, sections, sent, 0)
@@ -325,7 +340,7 @@
     f32, bf16 = jnp.float32, jnp.bfloat16
     return pl.pallas_call(
         functools.partial(stack_kernel, sections),
-        out_shape=jax.ShapeDtypeStruct(tokens_in.shape, tokens_in.dtype),
+        out_shape=pltpu.VMEM(tokens_in.shape, tokens_in.dtype),
         in_specs=[pl.BlockSpec(memory_space=pl.ANY)] * (1 + len(weights)),
         out_specs=pl.BlockSpec(memory_space=pltpu.VMEM),
         scratch_shapes=[
@@ -347,8 +362,9 @@
             vmem((sections, pair, length, width), bf16),
             pltpu.SemaphoreType.DMA((12,)),
             pltpu.SemaphoreType.DMA,
+            pltpu.SemaphoreType.DMA((sections, max(pair, stream_parts))),
             pltpu.SemaphoreType.DMA((sections, pair)),
-            pltpu.SemaphoreType.DMA((sections, pair)),
+            pltpu.SemaphoreType.DMA((sections, stream_parts)),
             pltpu.SemaphoreType.DMA,
         ],
         compiler_params=pltpu.CompilerParams(collective_id=0, has_side_effects=True),

time: 21 us -> 18.9 us (0.90)
  Pallas kernels: 19.4 us -> 18.1 us
  local copies, waits for them, and re-layouts: 1.38 us -> 0.62 us
    pallas_call x1, Pallas kernels: 19.4 us -> 18.1 us  [shards(): pl.pallas_call(functools.partial(stack_kernel, sections), out_shape=pltpu...]
    unnamed x1, local copies, waits for them, and re-layouts: 1.38 us -> 0.62 us
where the time goes in v3:
time: 18.9 us; the launch traced here: 18.7 us
  Pallas kernels  18.1 us (96%)
  local copies, waits for them, and re-layouts  0.62 us (3%)
    pallas_call x1, Pallas kernels, shards(): pl.pallas_call(functools.partial(stack_kernel, sections), out_shape=pltpu...  18.1 us
    unnamed x1, local copies, waits for them, and re-layouts  0.62 us

profile of v3, /device:TPU:17, one launch (start us, length us, event | category | flops | bytes accessed | tf_op | source)
XLA Modules:
  0.0 18.7 jit_solution(7183893981690263204)
XLA Ops:
  0.0 18.1 %section_stack.1 = bf16[1,1,8,2048]{3,2,1,0:T(8,128)(2,1)S(1)} custom-call(bf16[1,1,8,2048]{3,2,1,0:T(8,128)(2,1)} %tokens_hbm.1, bf16[1,2048,512]{2,1,0:T(8,128)(2,1)} %w_in_hbm.1, f32[1,4,512]{2,1,0:T(4,128)} %taps_hbm.1, f32[1,512]{1,0:T(1,128)} %cbias_hbm.1, bf16[1,8,64,64]{3,2,1,0:T(8,128)(2,1)} %grate_hbm.1, f32[1,512]{1,0:T(1,128)} %brate_hbm.1, ...), custom_call_target="tpu_custom_call" | custom-call | tf_op jit(solution)/shard_map/section_stack/pallas_call | solution.py:341
  18.1 0.6 %copy.14 = bf16[1,1,8,2048]{3,2,1,0:T(8,128)(2,1)} copy(bf16[1,1,8,2048]{3,2,1,0:T(8,128)(2,1)S(1)} %section_stack.1) | data formatting | bytes 65536
